TPU v7x, 32 devices: a whole 2x2x4 slice. The times are simulated.
32 devices in a mesh: gr: 2 (over y), sp: 4 (over z), tp: 4 (over x, core).
Axes of the slice: x: 2, y: 2, z: 4, core: 2. Of those that a mesh axis runs over, the one named last changes fastest.
Arguments:
- tokens: bfloat16 [4, 1024, 4096], P('gr', ('sp', 'tp')), parts along dimension 0, may hold values from -6 to 6
- norm_gain: bfloat16 [4096], replicated, may hold values from 0.099609375 to 1.8984375
- key_weight: bfloat16 [4096, 1024], P(None, 'tp'), may hold values from -0.09375 to 0.09375
- value_weight: bfloat16 [4096, 1024], P(None, 'tp'), may hold values from -0.09375 to 0.09375
- cum_gates: float32 [4, 1024, 16], P('gr', 'sp', 'tp'), parts along dimension 0, may hold values from -173 to 0, as said below
- new_query: bfloat16 [4, 1024], P('gr', 'tp'), parts along dimension 0, may hold values from -240 to 240
- new_key: bfloat16 [4, 1024], P('gr', 'tp'), parts along dimension 0, may hold values from -6 to 6
- new_value: bfloat16 [4, 1024], P('gr', 'tp'), parts along dimension 0, may hold values from -6 to 6
- new_gate: float32 [4, 16], P('gr', 'tp'), parts along dimension 0, may hold values from -5 to -1.5
Outputs:
- key_cache: bfloat16 [4, 1024, 1024], P('gr', 'sp', 'tp'), parts along dimension 0
- value_cache: bfloat16 [4, 1024, 1024], P('gr', 'sp', 'tp'), parts along dimension 0
- readout: bfloat16 [4, 1024], P('gr', 'tp'), parts along dimension 0
There are 2 independent parts, one for each index of `gr`. A program takes and returns all parts, laid end to end along the dimension named above; an argument that names none is the same for every part. Nothing has to cross between parts.
Inputs may be any that keep to these rules, and one draw needn't show every extreme that they name: `cum_gates`: along positions, for each prompt and head, the values never rise.
All inputs are finite; a program needn't handle non-finite values.
Results may differ from a plain program's by a relative error of at most 0.005.
The roundings to bfloat16 on the way count: a program that leaves them out, or rounds other values in their place, can miss the bound.
Values may be sent and summed in bfloat16 or wider, within the bound.
A program may use at most 64 MiB of HBM per device.

v0:
```python
import jax
import jax.numpy as jnp
from jax import lax
from jax.sharding import PartitionSpec as P

HD = 64
epsilon = 1e-06
masked_score = -1e30


def body(
    tokens, norm_gain, key_weight, value_weight, cum_gates, new_query, new_key, new_value, new_gate
):
    seq_count, own_len, model_width = tokens.shape
    as_float = tokens.astype(jnp.float32)
    normed = (
        as_float
        * lax.rsqrt(jnp.mean(as_float * as_float, axis=-1, keepdims=True) + epsilon)
        * norm_gain.astype(jnp.float32)
    ).astype(jnp.bfloat16)
    key_width = key_weight.shape[1]
    local_heads = key_width // HD
    both_weights = jnp.concatenate([key_weight, value_weight], axis=1)
    piece = lax.all_gather(normed, "tp", axis=1, tiled=True)
    piece_len = piece.shape[1]
    rows = piece.reshape(seq_count * piece_len, model_width)
    result = jnp.dot(rows, both_weights, preferred_element_type=jnp.float32).astype(jnp.bfloat16)
    projected = result.reshape(seq_count, piece_len, 2 * key_width)
    key_cache = projected[:, :, :key_width]
    value_cache = projected[:, :, key_width:]
    block_len = projected.shape[1]
    sp_count = lax.axis_size("sp")
    sp_index = lax.axis_index("sp")
    score_scale = HD ** (-0.5)
    queries = new_query.reshape(seq_count, local_heads, HD)
    fresh_key = new_key.reshape(seq_count, local_heads, HD).astype(jnp.float32)
    fresh_value = new_value.reshape(seq_count, local_heads, HD).astype(jnp.float32)
    fresh_score = jnp.sum(queries.astype(jnp.float32) * fresh_key, axis=-1) * score_scale
    key_heads = key_cache.reshape(seq_count, block_len, local_heads, HD)
    value_heads = value_cache.reshape(seq_count, block_len, local_heads, HD).astype(jnp.float32)
    scores = (
        jnp.einsum("shd,slhd->shl", queries, key_heads, preferred_element_type=jnp.float32)
        * score_scale
    )
    scores = scores - jnp.transpose(cum_gates, (0, 2, 1))
    last_block = sp_index == sp_count - 1
    fresh_term = jnp.where(
        last_block, fresh_score - (cum_gates[:, block_len - 1, :] + new_gate), masked_score
    )
    local_top = jnp.maximum(jnp.max(scores, axis=-1), fresh_term)
    maxima = lax.pmax(local_top, "sp")
    weights = jnp.exp(scores - maxima[:, :, None])
    fresh_weight = jnp.exp(fresh_term - maxima)
    totals = jnp.sum(weights, axis=-1) + fresh_weight
    weighted = jnp.einsum("shl,slhd->shd", weights, value_heads, precision=lax.Precision.HIGHEST)
    weighted = weighted + fresh_weight[:, :, None] * fresh_value
    totals, weighted = lax.psum((totals, weighted), "sp")
    readout = (weighted / totals[:, :, None]).reshape(seq_count, key_width).astype(jnp.bfloat16)
    return (key_cache, value_cache, readout)


def solution(mesh):
    in_specs = (
        P("gr", ("sp", "tp"), None),
        P(),
        P(None, "tp"),
        P(None, "tp"),
        P("gr", "sp", "tp"),
        P("gr", "tp"),
        P("gr", "tp"),
        P("gr", "tp"),
        P("gr", "tp"),
    )
    out_specs = (P("gr", "sp", "tp"), P("gr", "sp", "tp"), P("gr", "tp"))
    return jax.shard_map(body, mesh=mesh, in_specs=in_specs, out_specs=out_specs, check_vma=False)
```

profile of v0, /device:TPU:0, one launch (start us, length us, event | category | flops | bytes accessed | tf_op | source)
XLA Modules:
  0.0 83.7 jit_solution(6548077247722289311)
XLA Ops:
  7.2 0.0 all-gather.2.cloned.1.call-start
  7.2 0.7 convert_element_type.35
  7.9 1.7 %fusion.4 = f32[2,64]{1,0:T(2,128)S(1)} fusion(bf16[2,64,4096]{2,1,0:T(8,128)(2,1)} %param.9), kind=kLoop, calls=%fused_computation.6 | loop fusion | flops 1572736 | bytes 1049088 | tf_op jit(solution)/shard_map/reduce_sum | solution.py:18
  9.6 2.5 %fusion.6 = bf16[2,64,4096]{2,1,0:T(8,128)(2,1)} fusion(bf16[2,64,4096]{2,1,0:T(8,128)(2,1)} %param.9, f32[4096]{0:T(1024)S(1)} %convert_element_type.35, f32[2,64]{1,0:T(2,128)S(1)} %add_rsqrt_fusion), kind=kLoop, calls=%fused_computation.8 | loop fusion | flops 2097152 | bytes 2114048 | tf_op jit(solution)/shard_map/convert_element_type | solution.py:20
  12.2 0.0 all-gather.2.cloned.1.call-update
  12.2 0.1 reshape.53
  12.3 0.1 reshape.44
  12.4 0.1 reshape.46
  12.4 0.1 reshape.47
  12.5 0.2 slice_reduce_fusion
  12.7 0.1 multiply_reduce_fusion
  12.8 36.7 %all-gather.2.cloned.1.call-done = bf16[2,256,4096]{2,1,0:T(8,128)(2,1)} async-done(((bf16[2,64,4096]{2,1,0:T(8,128)(2,1)}), bf16[2,256,4096]{2,1,0:T(8,128)(2,1)}) %all-gather.2.cloned.1.call-update) | async-done | bytes 4194320 | tf_op jit(solution)/shard_map/all_gather | solution.py:24
  49.5 5.2 %fusion.7 = bf16[512,512]{1,0:T(8,128)(2,1)S(1)} fusion(bf16[512,4096]{1,0:T(8,128)(2,1)} %bitcast.34, bf16[4096,256]{1,0:T(8,128)(2,1)S(1)} %copy-done.7, bf16[4096,256]{1,0:T(8,128)(2,1)} %param.11), kind=kOutput, calls=%fused_computation.9 | convolution fusion | flops 2156134400 | bytes 8912896 | tf_op jit(solution)/shard_map/dot_general | solution.py:27
  54.8 0.1 copy.20
  55.0 0.1 fusion.19
  55.1 0.1 fusion.15
  55.2 11.7 %pmax.7 = f32[2,4]{1,0:T(2,128)S(1)} all-reduce(f32[2,4]{1,0:T(2,128)S(1)} %get-tuple-element.10), channel_id=1, replica_groups=mesh['gr'=2,'sp'=4,'tp'=4] {'sp'}, use_global_device_ids=true, to_apply=%region_3.4 | all-reduce | flops 8 | bytes 64 | tf_op jit(solution)/shard_map/pmax | solution.py:51
  66.9 0.2 fusion.12
  67.1 0.1 copy.21
  67.2 0.3 fusion.10
  67.5 0.1 multiply_add_fusion
  67.6 8.5 %all-reduce = (f32[2,4,64]{2,1,0:T(4,128)S(1)}, f32[2,4]{1,0:T(2,128)S(1)}) all-reduce(f32[2,4,64]{2,1,0:T(4,128)S(1)} %multiply_add_fusion, f32[2,4]{1,0:T(2,128)S(1)} %get-tuple-element.8), channel_id=1, replica_groups=mesh['gr'=2,'sp'=4,'tp'=4] {'sp'}, use_global_device_ids=true, to_apply=%region_4.5 | all-reduce | flops 520 | bytes 4160 | tf_op jit(solution)/shard_map/psum | solution.py:57
  76.1 0.1 divide_convert_fusion
  76.2 0.7 convert_element_type.44
  (20 shorter events, 0.1 us)
Async XLA Ops:
  7.2 42.3 %all-gather.2.cloned.1.call-start = ((), (), s32[]{:S(2)}) async-start(), calls=%async_computation | async-start | bytes 5242880 | tf_op jit(solution)/shard_map/all_gather | solution.py:24
  7.9 4.3 %copy-start.3 = (bf16[2,256]{1,0:T(2,128)(2,1)S(1)}, bf16[2,256]{1,0:T(2,128)(2,1)}, u32[]{:S(2)}) copy-start(bf16[2,256]{1,0:T(2,128)(2,1)} %param.14) | copy-start | bytes 3076
  7.9 4.4 %copy-start.4 = (bf16[2,256]{1,0:T(2,128)(2,1)S(1)}, bf16[2,256]{1,0:T(2,128)(2,1)}, u32[]{:S(2)}) copy-start(bf16[2,256]{1,0:T(2,128)(2,1)} %param.15) | copy-start | bytes 3076
  7.9 4.5 %copy-start.5 = (bf16[2,256]{1,0:T(2,128)(2,1)S(1)}, bf16[2,256]{1,0:T(2,128)(2,1)}, u32[]{:S(2)}) copy-start(bf16[2,256]{1,0:T(2,128)(2,1)} %param.16) | copy-start | bytes 3076
  7.9 4.6 %copy-start.2 = (f32[2,256,4]{1,2,0:T(4,128)S(1)}, f32[2,256,4]{1,2,0:T(4,128)}, u32[]{:S(2)}) copy-start(f32[2,256,4]{1,2,0:T(4,128)} %param.13) | copy-start | bytes 24580
  7.9 41.6 %copy-start.7 = (bf16[4096,256]{1,0:T(8,128)(2,1)S(1)}, bf16[4096,256]{1,0:T(8,128)(2,1)}, u32[]{:S(2)}) copy-start(bf16[4096,256]{1,0:T(8,128)(2,1)} %param.12) | copy-start | bytes 6291460
  49.5 5.7 %copy-start.6 = (f32[2,4]{1,0:T(2,128)S(1)}, f32[2,4]{1,0:T(2,128)}, u32[]{:S(2)}) copy-start(f32[2,4]{1,0:T(2,128)} %param.17) | copy-start | bytes 100
  54.8 22.1 %copy-start = (bf16[2,256,256]{2,1,0:T(8,128)(2,1)}, bf16[2,256,256]{2,1,0:T(8,128)(2,1)S(1)}, u32[]{:S(2)}) copy-start(bf16[2,256,256]{2,1,0:T(8,128)(2,1)S(1)} %get-tuple-element.12) | copy-start | bytes 786436
  54.8 22.0 %copy-start.1 = (bf16[2,256,256]{2,1,0:T(8,128)(2,1)}, bf16[2,256,256]{2,1,0:T(8,128)(2,1)S(1)}, u32[]{:S(2)}) copy-start(bf16[2,256,256]{2,1,0:T(8,128)(2,1)S(1)} %get-tuple-element.13) | copy-start | bytes 786436
Sparse Core Ops, SparseCore 0:
  12.3 37.1 all-gather.1
where the time goes:
time: 84 us; the launch traced here: 83.7 us
  waiting for transfers between devices  36.8 us (44%)
  blocking collectives  20.2 us (24%)
  between operations  14.1 us (17%)
  matrix products  5.69 us (7%)
  other arithmetic  5.42 us (6%)
  local copies, waits for them, and re-layouts  1.48 us (2%)
    all_gather x1, waiting for transfers between devices, body(): piece = lax.all_gather(normed, 'tp', axis=1, tiled=True)  36.7 us
    pmax x1, blocking collectives, body(): maxima = lax.pmax(local_top, 'sp')  11.7 us
    psum x1, blocking collectives, body(): totals, weighted = lax.psum((totals, weighted), 'sp')  8.5 us
    dot_general x1, matrix products, body(): jnp.dot(rows, both_weights, preferred_element_type=jnp.float32)  5.24 us
    convert_element_type x1, other arithmetic, body(): normed = (as_float * lax.rsqrt(jnp.mean(as_float * as_float, axis=-1, kee...  2.53 us
  transfers between devices with their start and end apart: 1, of which 1 were waited for; matrix products, arithmetic and copies ran while one was open for 1% of the time, Pallas kernels for 0%

commit v1 on v0

--- a/solution.py
+++ b/solution.py
@@ -21,7 +21,8 @@
     key_width = key_weight.shape[1]
     local_heads = key_width // HD
     both_weights = jnp.concatenate([key_weight, value_weight], axis=1)
-    piece = lax.all_gather(normed, "tp", axis=1, tiled=True)
+    sent = jnp.stack([normed] * lax.axis_size("tp"))
+    piece = jnp.concatenate(lax.all_to_all(sent, "tp", 0, 0), axis=1)
     piece_len = piece.shape[1]
     rows = piece.reshape(seq_count * piece_len, model_width)
     result = jnp.dot(rows, both_weights, preferred_element_type=jnp.float32).astype(jnp.bfloat16)

time: 84 us -> 89.5 us (1.065)
  between operations: 14.1 us -> 0.75 us
  waiting for transfers between devices: 36.8 us -> 48.3 us
  local copies, waits for them, and re-layouts: 1.48 us -> 6.8 us
  starting transfers between devices: 0.04 us -> 5 us
  matrix products: 5.69 us -> 2.77 us
  other arithmetic: 5.42 us -> 4.29 us
  blocking collectives: 20.2 us -> 21.3 us
    all_to_all x0 -> x1, waiting for transfers between devices: none -> 48.3 us  [body(): piece = jnp.concatenate(lax.all_to_all(sent, 'tp', 0, 0), axis=1)]
    all_gather x1 -> x0, waiting for transfers between devices: 36.7 us -> none  [body(): piece = lax.all_gather(normed, 'tp', axis=1, tiled=True)]
    all_to_all x0 -> x1, starting transfers between devices: none -> 5 us  [body(): piece = jnp.concatenate(lax.all_to_all(sent, 'tp', 0, 0), axis=1)]
    dot_general x1, matrix products: 5.24 us -> 2.32 us  [body(): jnp.dot(rows, both_weights, preferred_element_type=jnp.float32)]
    all_to_all x0 -> x1, local copies, waits for them, and re-layouts: none -> 2.61 us  [body(): piece = jnp.concatenate(lax.all_to_all(sent, 'tp', 0, 0), axis=1)]
    another operation x0 -> x1, local copies, waits for them, and re-layouts: none -> 2.48 us  [body(): sent = jnp.stack([normed] * lax.axis_size('tp'))]
    pmax x1, blocking collectives: 11.7 us -> 12.8 us  [body(): maxima = lax.pmax(local_top, 'sp')]
    convert_element_type x1, other arithmetic: 2.53 us -> 1.55 us  [body(): normed = (as_float * lax.rsqrt(jnp.mean(as_float * as_float, axis=-1, kee...]
where the time goes in v1:
time: 89.5 us; the launch traced here: 89.2 us
  waiting for transfers between devices  48.3 us (54%)
  blocking collectives  21.3 us (24%)
  local copies, waits for them, and re-layouts  6.8 us (8%)
  starting transfers between devices  5 us (6%)
  other arithmetic  4.29 us (5%)
  matrix products  2.77 us (3%)
    all_to_all x1, waiting for transfers between devices, body(): piece = jnp.concatenate(lax.all_to_all(sent, 'tp', 0, 0), axis=1)  48.3 us
    pmax x1, blocking collectives, body(): maxima = lax.pmax(local_top, 'sp')  12.8 us
    psum x1, blocking collectives, body(): totals, weighted = lax.psum((totals, weighted), 'sp')  8.5 us
    all_to_all x1, starting transfers between devices, body(): piece = jnp.concatenate(lax.all_to_all(sent, 'tp', 0, 0), axis=1)  5 us
    all_to_all x1, local copies, waits for them, and re-layouts, body(): piece = jnp.concatenate(lax.all_to_all(sent, 'tp', 0, 0), axis=1)  2.61 us
    another operation x1, local copies, waits for them, and re-layouts, body(): sent = jnp.stack([normed] * lax.axis_size('tp'))  2.48 us
    dot_general x1, matrix products, body(): jnp.dot(rows, both_weights, preferred_element_type=jnp.float32)  2.32 us
  transfers between devices with their start and end apart: 1, of which 1 were waited for; matrix products, arithmetic and copies ran while one was open for 1% of the time, Pallas kernels for 0%

profile of v1, /device:TPU:0, one launch (start us, length us, event | category | flops | bytes accessed | tf_op | source)
XLA Modules:
  0.0 89.2 jit_solution(17260342584295695094)
XLA Ops:
  0.6 0.7 convert_element_type.35
  1.3 1.5 %fusion.4 = f32[2,64]{1,0:T(2,128)S(1)} fusion(bf16[2,64,4096]{2,1,0:T(8,128)(2,1)} %param.9), kind=kLoop, calls=%fused_computation.6 | loop fusion | flops 1572736 | bytes 1049088 | tf_op jit(solution)/shard_map/reduce_sum | solution.py:18
  2.9 1.6 %fusion.6 = bf16[2,64,4096]{2,1,0:T(8,128)(2,1)S(1)} fusion(bf16[2,64,4096]{2,1,0:T(8,128)(2,1)} %param.9, f32[4096]{0:T(1024)S(1)} %convert_element_type.35, f32[2,64]{1,0:T(2,128)S(1)} %add_rsqrt_fusion), kind=kLoop, calls=%fused_computation.8 | loop fusion | flops 2097152 | bytes 2114048 | tf_op jit(solution)/shard_map/convert_element_type | solution.py:20
  4.4 2.5 %stack.2 = bf16[4,2,64,4096]{3,2,1,0:T(8,128)(2,1)} broadcast(bf16[2,64,4096]{2,1,0:T(8,128)(2,1)S(1)} %fusion.6), dimensions={1,2,3} | broadcast | bytes 5242880 | tf_op jit(solution)/shard_map/stack | solution.py:24
  6.9 5.0 %all-to-all-start = ((bf16[4,2,64,4096]{3,2,1,0:T(8,128)(2,1)}), bf16[4,2,64,4096]{3,2,1,0:T(8,128)(2,1)}, u32[]{:S(2)}, u32[]{:S(2)}) async-start(bf16[4,2,64,4096]{3,2,1,0:T(8,128)(2,1)} %stack.2), calls=%async_computation | async-start | bytes 8388608 | tf_op jit(solution)/shard_map/all_to_all | solution.py:25
  11.9 0.1 reshape.55
  12.0 0.1 reshape.46
  12.1 0.1 reshape.48
  12.2 0.1 reshape.49
  12.3 0.2 slice_reduce_fusion
  12.4 0.1 multiply_reduce_fusion
  12.5 48.3 %all-to-all-done = bf16[4,2,64,4096]{3,2,1,0:T(8,128)(2,1)} async-done(((bf16[4,2,64,4096]{3,2,1,0:T(8,128)(2,1)}), bf16[4,2,64,4096]{3,2,1,0:T(8,128)(2,1)}, u32[]{:S(2)}, u32[]{:S(2)}) %all-to-all-start) | async-done | bytes 4194336 | tf_op jit(solution)/shard_map/all_to_all | solution.py:25
  60.8 2.6 %copy.16 = bf16[4,2,64,4096]{3,2,0,1:T(8,128)(2,1)S(1)} copy(bf16[4,2,64,4096]{3,2,1,0:T(8,128)(2,1)} %all-to-all-done) | data formatting | bytes 8388608 | tf_op jit(solution)/shard_map/all_to_all | solution.py:25
  63.4 0.2 copy-done.8
  63.6 2.3 %fusion.7 = bf16[512,512]{1,0:T(8,128)(2,1)S(1)} fusion(bf16[512,4096]{1,0:T(8,128)(2,1)S(1)} %bitcast.32, bf16[4096,256]{1,0:T(8,128)(2,1)S(1)} %copy-done.7, bf16[4096,256]{1,0:T(8,128)(2,1)S(1)} %copy-done.8), kind=kOutput, calls=%fused_computation.9 | convolution fusion | flops 2156134400 | bytes 8912896 | tf_op jit(solution)/shard_map/dot_general | solution.py:28
  66.0 0.1 copy.25
  66.2 0.1 fusion.19
  66.3 0.1 fusion.15
  66.4 12.8 %pmax.7 = f32[2,4]{1,0:T(2,128)S(1)} all-reduce(f32[2,4]{1,0:T(2,128)S(1)} %get-tuple-element.13), channel_id=1, replica_groups=mesh['gr'=2,'sp'=4,'tp'=4] {'sp'}, use_global_device_ids=true, to_apply=%region_3.4 | all-reduce | flops 8 | bytes 64 | tf_op jit(solution)/shard_map/pmax | solution.py:52
  79.2 0.2 fusion.12
  79.4 0.1 copy.26
  79.5 0.3 fusion.10
  79.9 8.5 %all-reduce = (f32[2,4,64]{2,1,0:T(4,128)S(1)}, f32[2,4]{1,0:T(2,128)S(1)}) all-reduce(f32[2,4,64]{2,1,0:T(4,128)S(1)} %multiply_add_fusion, f32[2,4]{1,0:T(2,128)S(1)} %get-tuple-element.11), channel_id=1, replica_groups=mesh['gr'=2,'sp'=4,'tp'=4] {'sp'}, use_global_device_ids=true, to_apply=%region_4.5 | all-reduce | flops 520 | bytes 4160 | tf_op jit(solution)/shard_map/psum | solution.py:58
  88.5 0.7 convert_element_type.44
  (23 shorter events, 0.2 us)
Async XLA Ops:
  6.9 5.0 %copy-start.3 = (bf16[2,256]{1,0:T(2,128)(2,1)S(1)}, bf16[2,256]{1,0:T(2,128)(2,1)}, u32[]{:S(2)}) copy-start(bf16[2,256]{1,0:T(2,128)(2,1)} %param.14) | copy-start | bytes 3076
  6.9 5.2 %copy-start.4 = (bf16[2,256]{1,0:T(2,128)(2,1)S(1)}, bf16[2,256]{1,0:T(2,128)(2,1)}, u32[]{:S(2)}) copy-start(bf16[2,256]{1,0:T(2,128)(2,1)} %param.15) | copy-start | bytes 3076
  6.9 5.3 %copy-start.5 = (bf16[2,256]{1,0:T(2,128)(2,1)S(1)}, bf16[2,256]{1,0:T(2,128)(2,1)}, u32[]{:S(2)}) copy-start(bf16[2,256]{1,0:T(2,128)(2,1)} %param.16) | copy-start | bytes 3076
  6.9 5.4 %copy-start.2 = (f32[2,256,4]{1,2,0:T(4,128)S(1)}, f32[2,256,4]{1,2,0:T(4,128)}, u32[]{:S(2)}) copy-start(f32[2,256,4]{1,2,0:T(4,128)} %param.13) | copy-start | bytes 24580
  6.9 53.9 %all-to-all-start = ((bf16[4,2,64,4096]{3,2,1,0:T(8,128)(2,1)}), bf16[4,2,64,4096]{3,2,1,0:T(8,128)(2,1)}, u32[]{:S(2)}, u32[]{:S(2)}) async-start(bf16[4,2,64,4096]{3,2,1,0:T(8,128)(2,1)} %stack.2), calls=%async_computation | async-start | bytes 8388608 | tf_op jit(solution)/shard_map/all_to_all | solution.py:25
  12.5 50.9 %copy-start.7 = (bf16[4096,256]{1,0:T(8,128)(2,1)S(1)}, bf16[4096,256]{1,0:T(8,128)(2,1)}, u32[]{:S(2)}) copy-start(bf16[4096,256]{1,0:T(8,128)(2,1)} %param.12) | copy-start | bytes 6291460
  60.8 2.9 %copy-start.8 = (bf16[4096,256]{1,0:T(8,128)(2,1)S(1)}, bf16[4096,256]{1,0:T(8,128)(2,1)}, u32[]{:S(2)}) copy-start(bf16[4096,256]{1,0:T(8,128)(2,1)} %param.11) | copy-start | bytes 6291460
  63.6 2.8 %copy-start.6 = (f32[2,4]{1,0:T(2,128)S(1)}, f32[2,4]{1,0:T(2,128)}, u32[]{:S(2)}) copy-start(f32[2,4]{1,0:T(2,128)} %param.17) | copy-start | bytes 100
  66.0 23.1 %copy-start = (bf16[2,256,256]{2,1,0:T(8,128)(2,1)}, bf16[2,256,256]{2,1,0:T(8,128)(2,1)S(1)}, u32[]{:S(2)}) copy-start(bf16[2,256,256]{2,1,0:T(8,128)(2,1)S(1)} %get-tuple-element.15) | copy-start | bytes 786436
  66.0 23.1 %copy-start.1 = (bf16[2,256,256]{2,1,0:T(8,128)(2,1)}, bf16[2,256,256]{2,1,0:T(8,128)(2,1)S(1)}, u32[]{:S(2)}) copy-start(bf16[2,256,256]{2,1,0:T(8,128)(2,1)S(1)} %get-tuple-element.16) | copy-start | bytes 786436
